TPU v7x, 32 devices: a whole 2x2x4 slice. The times are simulated.
32 devices in a mesh: grp: 2 (over x), sp: 4 (over y, core), tp: 4 (over z).
Axes of the slice: x: 2, y: 2, z: 4, core: 2. Of those that a mesh axis runs over, the one named last changes fastest.
Arguments:
- layer_input: bfloat16 [8, 1024, 2048], P(('grp', 'tp'), 'sp'), parts along dimension 0, may hold values from -6 to 6
- norm_gain: bfloat16 [2048], replicated, may hold values from 0.099609375 to 1.8984375
- key_weight: bfloat16 [2048, 1024], replicated, may hold values from -0.125 to 0.125
- value_weight: bfloat16 [2048, 1024], replicated, may hold values from -0.125 to 0.125
- input_gate_weight: bfloat16 [2048, 8], replicated, may hold values from -0.125 to 0.125
- forget_gate_weight: bfloat16 [2048, 8], replicated, may hold values from -0.125 to 0.125
- conv_weight: float32 [4, 1024], replicated, may hold values from -3 to 3
- input_shift: float32 [8, 8, 1024], P(('grp', 'sp'), 'tp'), parts along dimension 0, may hold values from -4 to 302
- forget_shift: float32 [8, 8, 1024], P(('grp', 'sp'), 'tp'), parts along dimension 0, may hold values from 0 to 10.1
- new_query: bfloat16 [8, 8, 128], P(('grp', 'sp'), 'tp'), parts along dimension 0, may hold values from 0.1 to 2
- new_key: bfloat16 [8, 8, 128], P(('grp', 'sp'), 'tp'), parts along dimension 0, may hold values from -6 to 6
- new_value: bfloat16 [8, 8, 128], P(('grp', 'sp'), 'tp'), parts along dimension 0, may hold values from -6 to 6
- new_input: float32 [8, 8], P(('grp', 'sp'), 'tp'), parts along dimension 0, may hold values from 2 to 6
- new_forget: float32 [8, 8], P(('grp', 'sp'), 'tp'), parts along dimension 0, may hold values from -1 to 3
Outputs:
- key_cache: bfloat16 [8, 8, 1024, 128], P(('grp', 'sp'), 'tp'), parts along dimension 0
- value_cache: bfloat16 [8, 8, 1024, 128], P(('grp', 'sp'), 'tp'), parts along dimension 0
- weight_cache: float32 [8, 8, 1024], P(('grp', 'sp'), 'tp'), parts along dimension 0
- first_read: bfloat16 [8, 8, 128], P(('grp', 'sp'), 'tp'), parts along dimension 0
There are 2 independent parts, one for each index of `grp`. A program takes and returns all parts, laid end to end along the dimension named above; an argument that names none is the same for every part. Nothing has to cross between parts.
All inputs are finite; a program needn't handle non-finite values.
Results may differ from a plain program's by a relative error of at most 0.012.
Values may be sent and summed in bfloat16 or wider, within the bound.
A program may use at most 64 MiB of HBM per device.

v0:
```python
import jax
import jax.numpy as jnp
from jax import lax
from jax.sharding import PartitionSpec as P

HEADS = 8
DK = 128
CONV = 4


epsilon = 1e-06


def shifted(block, axis, distance):
    devices = range(lax.axis_size(axis))
    route = [(i - distance, i) for i in devices if i - distance in devices]
    return lax.ppermute(block, axis, route)


def project_rows(
    token_rows, norm_gain, key_weight, value_weight, input_gate_weight, forget_gate_weight
):
    widened = token_rows.astype(jnp.float32)
    normed = (
        widened
        * lax.rsqrt(jnp.mean(widened * widened, axis=-1, keepdims=True) + epsilon)
        * norm_gain.astype(jnp.float32)
    ).astype(jnp.bfloat16)
    key_matrix = key_weight.reshape(key_weight.shape[0], HEADS, DK)
    value_matrix = value_weight.reshape(value_weight.shape[0], HEADS, DK)
    key_linear = jnp.einsum(
        "apd,dhk->ahpk", normed, key_matrix, preferred_element_type=jnp.float32
    ).astype(jnp.bfloat16)
    values = jnp.einsum(
        "apd,dhk->ahpk", normed, value_matrix, preferred_element_type=jnp.float32
    ).astype(jnp.bfloat16)
    input_linear = jnp.einsum(
        "apd,dh->ahp", normed, input_gate_weight, preferred_element_type=jnp.float32
    ).astype(jnp.bfloat16)
    forget_linear = jnp.einsum(
        "apd,dh->ahp", normed, forget_gate_weight, preferred_element_type=jnp.float32
    ).astype(jnp.bfloat16)
    return (key_linear, values, input_linear, forget_linear)


def convolve(key_linear, previous, conv_weight):
    extended = jnp.concatenate([previous, key_linear], axis=2).astype(jnp.float32)
    length = key_linear.shape[2]
    tap_weight = conv_weight.reshape(CONV, HEADS, 1, DK)
    summed = extended[:, :, 0:length, :] * tap_weight[0]
    for offset in range(1, CONV):
        summed = summed + extended[:, :, offset : offset + length, :] * tap_weight[offset]
    return jax.nn.silu(summed).astype(jnp.bfloat16)


def read_cache(
    keys,
    values,
    input_linear,
    forget_linear,
    input_shift,
    forget_shift,
    new_query,
    new_key,
    new_value,
    new_input,
    new_forget,
):
    scaling = DK ** (-0.5)
    log_forget = jax.nn.log_sigmoid(forget_linear.astype(jnp.float32) + forget_shift)
    suffix = lax.cumsum(log_forget, axis=2, reverse=True) - log_forget
    new_decay = jax.nn.log_sigmoid(new_forget)
    log_weight = input_linear.astype(jnp.float32) + input_shift + suffix + new_decay[:, :, None]
    largest = jnp.maximum(jnp.max(log_weight, axis=2), new_input)
    weight_cache = jnp.exp(log_weight - largest[:, :, None])
    new_weight = jnp.exp(new_input - largest)
    matched = jnp.einsum("bhlk,bhk->bhl", keys, new_query, preferred_element_type=jnp.float32)
    scores = (weight_cache * matched * scaling).astype(jnp.bfloat16)
    fresh_match = jnp.sum(new_key.astype(jnp.float32) * new_query.astype(jnp.float32), axis=2)
    new_score = (new_weight * fresh_match * scaling).astype(jnp.bfloat16)
    denominator = jnp.sum(scores.astype(jnp.float32), axis=2) + new_score.astype(jnp.float32)
    numerator = jnp.einsum("bhl,bhlk->bhk", scores, values, preferred_element_type=jnp.float32)
    numerator = numerator + new_score.astype(jnp.float32)[:, :, None] * new_value.astype(
        jnp.float32
    )
    first_read = (numerator / jnp.maximum(jnp.abs(denominator), 1.0)[:, :, None]).astype(
        jnp.bfloat16
    )
    return (weight_cache, first_read)


def shards(
    layer_input,
    norm_gain,
    key_weight,
    value_weight,
    input_gate_weight,
    forget_gate_weight,
    conv_weight,
    input_shift,
    forget_shift,
    new_query,
    new_key,
    new_value,
    new_input,
    new_forget,
):
    key_linear, values, input_linear, forget_linear = project_rows(
        layer_input, norm_gain, key_weight, value_weight, input_gate_weight, forget_gate_weight
    )
    previous = shifted(key_linear[:, :, -(CONV - 1) :, :], "sp", 1)
    keys = convolve(key_linear, previous, conv_weight)
    keys, values, input_linear, forget_linear = (
        lax.all_to_all(
            lax.all_to_all(keys, "tp", split_axis=1, concat_axis=0, tiled=True),
            "sp",
            split_axis=0,
            concat_axis=2,
            tiled=True,
        ),
        lax.all_to_all(
            lax.all_to_all(values, "tp", split_axis=1, concat_axis=0, tiled=True),
            "sp",
            split_axis=0,
            concat_axis=2,
            tiled=True,
        ),
        lax.all_to_all(
            lax.all_to_all(input_linear, "tp", split_axis=1, concat_axis=0, tiled=True),
            "sp",
            split_axis=0,
            concat_axis=2,
            tiled=True,
        ),
        lax.all_to_all(
            lax.all_to_all(forget_linear, "tp", split_axis=1, concat_axis=0, tiled=True),
            "sp",
            split_axis=0,
            concat_axis=2,
            tiled=True,
        ),
    )
    weight_cache, first_read = read_cache(
        keys,
        values,
        input_linear,
        forget_linear,
        input_shift,
        forget_shift,
        new_query,
        new_key,
        new_value,
        new_input,
        new_forget,
    )
    return (keys, values, weight_cache, first_read)


def solution(mesh):
    in_specs = (
        P(("grp", "tp"), "sp", None),
        P(),
        P(),
        P(),
        P(),
        P(),
        P(),
        P(("grp", "sp"), "tp", None),
        P(("grp", "sp"), "tp", None),
        P(("grp", "sp"), "tp", None),
        P(("grp", "sp"), "tp", None),
        P(("grp", "sp"), "tp", None),
        P(("grp", "sp"), "tp"),
        P(("grp", "sp"), "tp"),
    )
    out_specs = (
        P(("grp", "sp"), "tp", None, None),
        P(("grp", "sp"), "tp", None, None),
        P(("grp", "sp"), "tp", None),
        P(("grp", "sp"), "tp", None),
    )
    return jax.shard_map(shards, mesh=mesh, in_specs=in_specs, out_specs=out_specs, check_vma=False)
```

profile of v0, /device:TPU:0, one launch (start us, length us, event | category | flops | bytes accessed | tf_op | source)
XLA Modules:
  0.0 106.6 jit_solution(14466072062410166473)
XLA Ops:
  0.6 0.0 copy-start
  0.6 0.0 copy-start.3
  0.7 0.0 copy-start.10
  0.7 0.8 convert_element_type.131
  1.4 1.5 %fusion.6 = f32[256]{0:T(256)S(1)} fusion(bf16[1,256,2048]{2,1,0:T(8,128)(2,1)} %param.14), kind=kLoop, calls=%fused_computation.8 | loop fusion | flops 1572608 | bytes 1049600 | tf_op jit(solution)/shard_map/reduce_sum | solution.py:26
  3.0 0.0 copy-done
  3.0 1.7 %fusion.22 = bf16[1,8,256]{2,1,0:T(8,128)(2,1)S(1)} fusion(bf16[2048,8]{0,1:T(8,128)(2,1)S(1)} %copy-done, bf16[1,256,2048]{2,1,0:T(8,128)(2,1)} %param.14, f32[2048]{0:T(1024)S(1)} %convert_element_type.131, f32[256]{0:T(256)S(1)} %add_rsqrt_fusion), kind=kOutput, calls=%fused_computation.18 | convolution fusion | flops 10487808 | bytes 1094656 | tf_op jit(solution)/shard_map/apd,dh->ahp/dot_general | solution.py:40
  4.7 0.5 broadcast.50
  5.2 0.7 reduce.10
  5.9 0.6 reshape.225
  6.5 6.3 %all-to-all-start.6 = ((bf16[4,2,256]{2,1,0:T(2,128)(2,1)}), bf16[4,2,256]{2,1,0:T(2,128)(2,1)S(1)}, u32[]{:S(2)}, u32[]{:S(2)}) async-start(bf16[4,2,256]{2,1,0:T(2,128)(2,1)} %reshape.225), calls=%async_computation.6 | async-start | bytes 8192 | tf_op jit(solution)/shard_map/all_to_all | solution.py:136
  12.8 0.0 copy-done.3
  12.8 0.0 copy-done.10
  12.8 0.4 fusion.21
  13.3 0.7 reduce.11
  14.0 0.6 reshape.227
  14.6 3.8 %all-to-all-done.6 = bf16[4,2,256]{2,1,0:T(2,128)(2,1)S(1)} async-done(((bf16[4,2,256]{2,1,0:T(2,128)(2,1)}), bf16[4,2,256]{2,1,0:T(2,128)(2,1)S(1)}, u32[]{:S(2)}, u32[]{:S(2)}) %all-to-all-start.6) | async-done | bytes 4128 | tf_op jit(solution)/shard_map/all_to_all | solution.py:136
  18.4 3.2 %all-to-all-start.4 = ((bf16[4,2,256]{2,1,0:T(2,128)(2,1)}), bf16[4,2,256]{2,1,0:T(2,128)(2,1)S(1)}, u32[]{:S(2)}, u32[]{:S(2)}) async-start(bf16[4,2,256]{2,1,0:T(2,128)(2,1)} %reshape.227), calls=%async_computation.4 | async-start | bytes 8192 | tf_op jit(solution)/shard_map/all_to_all | solution.py:129
  21.7 0.6 all_to_all.92
  22.3 4.9 %all-to-all-done.4 = bf16[4,2,256]{2,1,0:T(2,128)(2,1)S(1)} async-done(((bf16[4,2,256]{2,1,0:T(2,128)(2,1)}), bf16[4,2,256]{2,1,0:T(2,128)(2,1)S(1)}, u32[]{:S(2)}, u32[]{:S(2)}) %all-to-all-start.4) | async-done | bytes 4128 | tf_op jit(solution)/shard_map/all_to_all | solution.py:129
  27.2 3.2 %all-to-all-start.7 = ((bf16[4,2,256]{2,1,0:T(2,128)(2,1)}), bf16[4,2,256]{2,1,0:T(2,128)(2,1)S(1)}, u32[]{:S(2)}, u32[]{:S(2)}) async-start(bf16[4,2,256]{2,1,0:T(2,128)(2,1)} %all_to_all.92), calls=%async_computation.7 | async-start | bytes 8192 | tf_op jit(solution)/shard_map/all_to_all | solution.py:135
  30.5 0.6 all_to_all.89
  31.1 3.1 %all-to-all-done.7 = bf16[4,2,256]{2,1,0:T(2,128)(2,1)S(1)} async-done(((bf16[4,2,256]{2,1,0:T(2,128)(2,1)}), bf16[4,2,256]{2,1,0:T(2,128)(2,1)S(1)}, u32[]{:S(2)}, u32[]{:S(2)}) %all-to-all-start.7) | async-done | bytes 4128 | tf_op jit(solution)/shard_map/all_to_all | solution.py:135
  34.2 3.2 %all-to-all-start.5 = ((bf16[4,2,256]{2,1,0:T(2,128)(2,1)}), bf16[4,2,256]{2,1,0:T(2,128)(2,1)S(1)}, u32[]{:S(2)}, u32[]{:S(2)}) async-start(bf16[4,2,256]{2,1,0:T(2,128)(2,1)} %all_to_all.89), calls=%async_computation.5 | async-start | bytes 8192 | tf_op jit(solution)/shard_map/all_to_all | solution.py:128
  37.5 4.3 %fusion.15 = bf16[1,8,256,128]{3,2,0,1:T(8,128)(2,1)} fusion(bf16[1,256,2048]{2,1,0:T(8,128)(2,1)S(1)} %copy-done.3, f32[2048]{0:T(1024)S(1)} %convert_element_type.131, f32[256]{0:T(256)S(1)} %add_rsqrt_fusion, bf16[2048,1024]{1,0:T(8,128)(2,1)} %param.17), kind=kOutput, calls=%fused_computation.13 | convolution fusion | flops 1076101120 | bytes 5776384 | tf_op jit(solution)/shard_map/apd,dhk->ahpk/dot_general | solution.py:34
  41.8 0.0 all-to-all-done.5
  41.8 4.1 %all-to-all-start.2 = ((bf16[1,8,256,128]{3,2,0,1:T(8,128)(2,1)}), bf16[1,8,256,128]{3,2,0,1:T(8,128)(2,1)}, u32[]{:S(2)}, u32[]{:S(2)}) async-start(bf16[1,8,256,128]{3,2,0,1:T(8,128)(2,1)} %fusion.15), calls=%async_computation.2 | async-start | bytes 1048576 | tf_op jit(solution)/shard_map/all_to_all | solution.py:122
  45.9 0.0 copy-start.5
  45.9 3.5 %fusion.18 = bf16[1,8,256,128]{3,2,1,0:T(8,128)(2,1)S(1)} fusion(bf16[1,256,2048]{2,1,0:T(8,128)(2,1)S(1)} %copy-done.3, f32[2048]{0:T(1024)S(1)} %convert_element_type.131, f32[256]{0:T(256)S(1)} %add_rsqrt_fusion, bf16[2048,1024]{1,0:T(8,128)(2,1)} %param.16), kind=kOutput, calls=%fused_computation.14 | convolution fusion | flops 1076101120 | bytes 5776384 | tf_op jit(solution)/shard_map/apd,dhk->ahpk/dot_general | solution.py:31
  49.4 2.4 %collective-permute-start = (bf16[1,8,3,128]{3,2,1,0:T(4,128)(2,1)S(1)}, bf16[1,8,3,128]{3,2,1,0:T(4,128)(2,1)S(1)}, u32[]{:S(2)}, u32[]{:S(2)}) collective-permute-start(bf16[1,8,3,128]{3,2,1,0:T(4,128)(2,1)S(1)} %slice.48), channel_id=1, source_target_pairs={{0,4},{4,8},{8,12},{1,5},{5,9},{9,13},{2,6},{6,10},{10,14},{3,7},{... | collective-permute-start | bytes 18440 | tf_op jit(solution)/shard_map/ppermute | solution.py:17
  51.8 0.0 copy-done.5
  51.8 0.8 collective-permute-done
  52.6 0.1 maximum_convert_fusion
  52.7 0.0 copy-start.7
  52.7 0.0 copy-start.11
  52.8 0.0 copy-start.12
  52.8 0.0 copy-start.4
  52.8 1.5 %fusion.30 = bf16[1,8,256,128]{3,2,0,1:T(8,128)(2,1)} fusion(f32[8,128]{1,0:T(8,128)S(1)} %bitcast.172, f32[1,8,259,128]{3,2,1,0:T(8,128)S(1)} %maximum_convert_fusion, f32[8,128]{1,0:T(8,128)S(1)} %bitcast.173, f32[8,128]{1,0:T(8,128)S(1)} %bitcast.171, f32[8,128]{1,0:T(8,128)S(1)} %bitcast.170), kind=kLoop, calls=%fused_computation.32 | loop fusion | flops 3145728 | bytes 4734976 | tf_op jit(solution)/shard_map/convert_element_type | solution.py:53
  54.2 7.1 %all-to-all-done.2 = bf16[1,8,256,128]{3,2,0,1:T(8,128)(2,1)} async-done(((bf16[1,8,256,128]{3,2,0,1:T(8,128)(2,1)}), bf16[1,8,256,128]{3,2,0,1:T(8,128)(2,1)}, u32[]{:S(2)}, u32[]{:S(2)}) %all-to-all-start.2) | async-done | bytes 524320 | tf_op jit(solution)/shard_map/all_to_all | solution.py:122
  61.4 4.1 %all-to-all-start = ((bf16[1,8,256,128]{3,2,0,1:T(8,128)(2,1)}), bf16[1,8,256,128]{3,2,0,1:T(8,128)(2,1)}, u32[]{:S(2)}, u32[]{:S(2)}) async-start(bf16[1,8,256,128]{3,2,0,1:T(8,128)(2,1)} %fusion.30), calls=%async_computation | async-start | bytes 1048576 | tf_op jit(solution)/shard_map/all_to_all | solution.py:115
  65.5 0.0 copy-done.7
  65.5 0.0 copy-done.11
  65.5 0.1 multiply_reduce_fusion
  65.6 0.0 copy-done.12
  65.7 0.0 copy-done.4
  65.7 2.5 %reduce-window.6 = f32[1,2,8,128]{3,2,1,0:T(8,128)S(1)} reduce-window(f32[1,2,8,128]{3,2,1,0:T(8,128)S(1)} %copy.82, f32[]{:T(128)} %constant.7.clone.1), window={size=1x1x1x128 pad=0_0x0_0x0_0x0_127}, to_apply=%region_1.2 | reduce-window | flops 260096 | bytes 16388 | tf_op jit(solution)/shard_map/reduce-window
  68.2 0.1 slice_reduce_fusion
  68.3 0.2 reduce-window.9
  68.5 11.6 %all-to-all-done = bf16[1,8,256,128]{3,2,0,1:T(8,128)(2,1)} async-done(((bf16[1,8,256,128]{3,2,0,1:T(8,128)(2,1)}), bf16[1,8,256,128]{3,2,0,1:T(8,128)(2,1)}, u32[]{:S(2)}, u32[]{:S(2)}) %all-to-all-start) | async-done | bytes 524320 | tf_op jit(solution)/shard_map/all_to_all | solution.py:115
  80.1 3.5 %all-to-all-start.3 = ((bf16[4,2,256,128]{3,2,1,0:T(8,128)(2,1)}), bf16[4,2,256,128]{3,2,1,0:T(8,128)(2,1)S(1)}, u32[]{:S(2)}, u32[]{:S(2)}) async-start(bf16[4,2,256,128]{3,2,1,0:T(8,128)(2,1)} %bitcast.18), calls=%async_computation.3 | async-start | bytes 1048576 | tf_op jit(solution)/shard_map/all_to_all | solution.py:121
  83.6 0.1 slice_bitcast_fusion
  83.6 0.1 broadcast.41
  83.7 8.6 %all-to-all-done.3 = bf16[4,2,256,128]{3,2,1,0:T(8,128)(2,1)S(1)} async-done(((bf16[4,2,256,128]{3,2,1,0:T(8,128)(2,1)}), bf16[4,2,256,128]{3,2,1,0:T(8,128)(2,1)S(1)}, u32[]{:S(2)}, u32[]{:S(2)}) %all-to-all-start.3) | async-done | bytes 524320 | tf_op jit(solution)/shard_map/all_to_all | solution.py:121
  92.3 3.6 %all-to-all-start.1 = ((bf16[4,2,256,128]{3,2,1,0:T(8,128)(2,1)}), bf16[4,2,256,128]{3,2,1,0:T(8,128)(2,1)S(1)}, u32[]{:S(2)}, u32[]{:S(2)}) async-start(bf16[4,2,256,128]{3,2,1,0:T(8,128)(2,1)} %bitcast.10), calls=%async_computation.1 | async-start | bytes 1048576 | tf_op jit(solution)/shard_map/all_to_all | solution.py:114
  96.0 0.0 copy-done.6
  96.0 0.2 fusion.55
  96.2 0.0 copy-done.8
  96.2 0.0 copy-start.1
  96.2 8.5 %all-to-all-done.1 = bf16[4,2,256,128]{3,2,1,0:T(8,128)(2,1)S(1)} async-done(((bf16[4,2,256,128]{3,2,1,0:T(8,128)(2,1)}), bf16[4,2,256,128]{3,2,1,0:T(8,128)(2,1)S(1)}, u32[]{:S(2)}, u32[]{:S(2)}) %all-to-all-start.1) | async-done | bytes 524320 | tf_op jit(solution)/shard_map/all_to_all | solution.py:114
  104.8 0.0 copy-start.2
  104.8 0.2 fusion.36
  105.0 0.8 convert_reduce_fusion
  105.8 0.2 fusion.34
  106.0 0.6 fusion.38
  (26 shorter events, 0.3 us)
Async XLA Ops:
  0.6 2.3 %copy-start = (bf16[2048,8]{0,1:T(8,128)(2,1)S(1)}, bf16[2048,8]{0,1:T(8,128)(2,1)}, u32[]{:S(2)}) copy-start(bf16[2048,8]{0,1:T(8,128)(2,1)} %param.19) | copy-start | bytes 98308
  0.6 12.2 %copy-start.3 = (bf16[1,256,2048]{2,1,0:T(8,128)(2,1)S(1)}, bf16[1,256,2048]{2,1,0:T(8,128)(2,1)}, u32[]{:S(2)}) copy-start(bf16[1,256,2048]{2,1,0:T(8,128)(2,1)} %param.14) | copy-start | bytes 3145732
  0.7 12.2 %copy-start.10 = (bf16[2048,8]{0,1:T(8,128)(2,1)S(1)}, bf16[2048,8]{0,1:T(8,128)(2,1)}, u32[]{:S(2)}) copy-start(bf16[2048,8]{0,1:T(8,128)(2,1)} %param.18) | copy-start | bytes 98308
  6.5 11.9 %all-to-all-start.6 = ((bf16[4,2,256]{2,1,0:T(2,128)(2,1)}), bf16[4,2,256]{2,1,0:T(2,128)(2,1)S(1)}, u32[]{:S(2)}, u32[]{:S(2)}) async-start(bf16[4,2,256]{2,1,0:T(2,128)(2,1)} %reshape.225), calls=%async_computation.6 | async-start | bytes 8192 | tf_op jit(solution)/shard_map/all_to_all | solution.py:136
  18.4 8.8 %all-to-all-start.4 = ((bf16[4,2,256]{2,1,0:T(2,128)(2,1)}), bf16[4,2,256]{2,1,0:T(2,128)(2,1)S(1)}, u32[]{:S(2)}, u32[]{:S(2)}) async-start(bf16[4,2,256]{2,1,0:T(2,128)(2,1)} %reshape.227), calls=%async_computation.4 | async-start | bytes 8192 | tf_op jit(solution)/shard_map/all_to_all | solution.py:129
  27.2 7.0 %all-to-all-start.7 = ((bf16[4,2,256]{2,1,0:T(2,128)(2,1)}), bf16[4,2,256]{2,1,0:T(2,128)(2,1)S(1)}, u32[]{:S(2)}, u32[]{:S(2)}) async-start(bf16[4,2,256]{2,1,0:T(2,128)(2,1)} %all_to_all.92), calls=%async_computation.7 | async-start | bytes 8192 | tf_op jit(solution)/shard_map/all_to_all | solution.py:135
  34.2 7.5 %all-to-all-start.5 = ((bf16[4,2,256]{2,1,0:T(2,128)(2,1)}), bf16[4,2,256]{2,1,0:T(2,128)(2,1)S(1)}, u32[]{:S(2)}, u32[]{:S(2)}) async-start(bf16[4,2,256]{2,1,0:T(2,128)(2,1)} %all_to_all.89), calls=%async_computation.5 | async-start | bytes 8192 | tf_op jit(solution)/shard_map/all_to_all | solution.py:128
  41.8 19.6 %all-to-all-start.2 = ((bf16[1,8,256,128]{3,2,0,1:T(8,128)(2,1)}), bf16[1,8,256,128]{3,2,0,1:T(8,128)(2,1)}, u32[]{:S(2)}, u32[]{:S(2)}) async-start(bf16[1,8,256,128]{3,2,0,1:T(8,128)(2,1)} %fusion.15), calls=%async_computation.2 | async-start | bytes 1048576 | tf_op jit(solution)/shard_map/all_to_all | solution.py:122
  45.9 5.9 %copy-start.5 = (f32[4,1024]{1,0:T(4,128)S(1)}, f32[4,1024]{1,0:T(4,128)}, u32[]{:S(2)}) copy-start(f32[4,1024]{1,0:T(4,128)} %param.20) | copy-start | bytes 49156
  49.4 3.2 %collective-permute-start = (bf16[1,8,3,128]{3,2,1,0:T(4,128)(2,1)S(1)}, bf16[1,8,3,128]{3,2,1,0:T(4,128)(2,1)S(1)}, u32[]{:S(2)}, u32[]{:S(2)}) collective-permute-start(bf16[1,8,3,128]{3,2,1,0:T(4,128)(2,1)S(1)} %slice.48), channel_id=1, source_target_pairs={{0,4},{4,8},{8,12},{1,5},{5,9},{9,13},{2,6},{6,10},{10,14},{3,7},{... | collective-permute-start | bytes 18440 | tf_op jit(solution)/shard_map/ppermute | solution.py:17
  52.7 12.8 %copy-start.7 = (bf16[1,2,128]{2,1,0:T(2,128)(2,1)S(1)}, bf16[1,2,128]{2,1,0:T(2,128)(2,1)}, u32[]{:S(2)}) copy-start(bf16[1,2,128]{2,1,0:T(2,128)(2,1)} %param.23) | copy-start | bytes 1540
  52.7 12.8 %copy-start.11 = (bf16[1,2,128]{2,1,0:T(2,128)(2,1)S(1)}, bf16[1,2,128]{2,1,0:T(2,128)(2,1)}, u32[]{:S(2)}) copy-start(bf16[1,2,128]{2,1,0:T(2,128)(2,1)} %param.24) | copy-start | bytes 1540
  52.8 12.9 %copy-start.12 = (f32[1,2]{1,0:T(1,128)S(1)}, f32[1,2]{1,0:T(1,128)}, u32[]{:S(2)}) copy-start(f32[1,2]{1,0:T(1,128)} %param.27) | copy-start | bytes 28
  52.8 12.9 %copy-start.4 = (f32[1,2,1024]{2,1,0:T(2,128)S(1)}, f32[1,2,1024]{2,1,0:T(2,128)}, u32[]{:S(2)}) copy-start(f32[1,2,1024]{2,1,0:T(2,128)} %param.22) | copy-start | bytes 24580
  54.2 41.7 %copy-start.6 = (f32[1,2,1024]{2,1,0:T(2,128)S(1)}, f32[1,2,1024]{2,1,0:T(2,128)}, u32[]{:S(2)}) copy-start(f32[1,2,1024]{2,1,0:T(2,128)} %param.21) | copy-start | bytes 24580
  54.2 41.9 %copy-start.8 = (f32[1,2]{1,0:T(1,128)S(1)}, f32[1,2]{1,0:T(1,128)}, u32[]{:S(2)}) copy-start(f32[1,2]{1,0:T(1,128)} %param.26) | copy-start | bytes 28
  61.4 18.7 %all-to-all-start = ((bf16[1,8,256,128]{3,2,0,1:T(8,128)(2,1)}), bf16[1,8,256,128]{3,2,0,1:T(8,128)(2,1)}, u32[]{:S(2)}, u32[]{:S(2)}) async-start(bf16[1,8,256,128]{3,2,0,1:T(8,128)(2,1)} %fusion.30), calls=%async_computation | async-start | bytes 1048576 | tf_op jit(solution)/shard_map/all_to_all | solution.py:115
  80.1 12.3 %all-to-all-start.3 = ((bf16[4,2,256,128]{3,2,1,0:T(8,128)(2,1)}), bf16[4,2,256,128]{3,2,1,0:T(8,128)(2,1)S(1)}, u32[]{:S(2)}, u32[]{:S(2)}) async-start(bf16[4,2,256,128]{3,2,1,0:T(8,128)(2,1)} %bitcast.18), calls=%async_computation.3 | async-start | bytes 1048576 | tf_op jit(solution)/shard_map/all_to_all | solution.py:121
  92.3 13.7 %copy-start.9 = (bf16[1,2,128]{2,1,0:T(2,128)(2,1)S(1)}, bf16[1,2,128]{2,1,0:T(2,128)(2,1)}, u32[]{:S(2)}) copy-start(bf16[1,2,128]{2,1,0:T(2,128)(2,1)} %param.25) | copy-start | bytes 1540
  92.3 12.4 %all-to-all-start.1 = ((bf16[4,2,256,128]{3,2,1,0:T(8,128)(2,1)}), bf16[4,2,256,128]{3,2,1,0:T(8,128)(2,1)S(1)}, u32[]{:S(2)}, u32[]{:S(2)}) async-start(bf16[4,2,256,128]{3,2,1,0:T(8,128)(2,1)} %bitcast.10), calls=%async_computation.1 | async-start | bytes 1048576 | tf_op jit(solution)/shard_map/all_to_all | solution.py:114
  96.2 10.4 %copy-start.1 = (bf16[4,2,256,128]{3,2,0,1:T(8,128)(2,1)}, bf16[4,2,256,128]{3,2,0,1:T(8,128)(2,1)S(1)}, u32[]{:S(2)}) copy-start(bf16[4,2,256,128]{3,2,0,1:T(8,128)(2,1)S(1)} %copy.45) | copy-start | bytes 1572868
  104.8 1.9 %copy-start.2 = (bf16[4,2,256,128]{3,2,0,1:T(8,128)(2,1)}, bf16[4,2,256,128]{3,2,0,1:T(8,128)(2,1)S(1)}, u32[]{:S(2)}) copy-start(bf16[4,2,256,128]{3,2,0,1:T(8,128)(2,1)S(1)} %copy.42) | copy-start | bytes 1572868
where the time goes:
time: 107 us
  waiting for transfers between devices  48.4 us (45%)
  starting transfers between devices  33.8 us (32%)
  matrix products  10.3 us (10%)
  other arithmetic  9.68 us (9%)
  local copies, waits for them, and re-layouts  3.49 us (3%)
    all_to_all x1, waiting for transfers between devices, shards(): lax.all_to_all(keys, 'tp', split_axis=1, concat_axis=0, tiled=True)  11.6 us
    all_to_all x1, waiting for transfers between devices, shards(): lax.all_to_all(lax.all_to_all(values, 'tp', split_axis=1, concat_axis=0,...  8.61 us
    all_to_all x1, waiting for transfers between devices, shards(): lax.all_to_all(lax.all_to_all(keys, 'tp', split_axis=1, concat_axis=0, ti...  8.51 us
    all_to_all x1, waiting for transfers between devices, shards(): lax.all_to_all(values, 'tp', split_axis=1, concat_axis=0, tiled=True)  7.12 us
    all_to_all x1, starting transfers between devices, shards(): lax.all_to_all(forget_linear, 'tp', split_axis=1, concat_axis=0, tiled=True)  6.35 us
    all_to_all x1, waiting for transfers between devices, shards(): lax.all_to_all(input_linear, 'tp', split_axis=1, concat_axis=0, tiled=True)  4.89 us
    dot_general x1, matrix products, project_rows(): jnp.einsum('apd,dhk->ahpk', normed, value_matrix, preferred_element_type=...  4.29 us
    all_to_all x1, starting transfers between devices, shards(): lax.all_to_all(values, 'tp', split_axis=1, concat_axis=0, tiled=True)  4.14 us
  transfers between devices with their start and end apart: 9, of which 8 were waited for; matrix products, arithmetic and copies ran while one was open for 14% of the time, Pallas kernels for 0%

commit v1 on v0

v1 whole, which is shorter than its diff:
```python
import functools

import jax
import jax.numpy as jnp
from jax import lax
from jax.experimental import pallas as pl
from jax.experimental.pallas import tpu as pltpu
from jax.sharding import PartitionSpec as P

MESH = pl.DeviceIdType.MESH
epsilon = 1e-06
SPLIT = 2


def log_sigmoid(x):
    return jnp.minimum(x, 0.0) - jnp.log1p(jnp.exp(-jnp.abs(x)))


def kernel(
    dims,
    x_ref,
    gain_ref,
    wi_ref,
    wf_ref,
    conv_ref,
    ishift_ref,
    fshift_ref,
    query_ref,
    nkey_ref,
    nvalue_ref,
    ninput_ref,
    nforget_ref,
    wk_ref,
    wv_ref,
    keys_out,
    values_out,
    weight_out,
    read_out,
    wbuf,
    normed,
    comp,
    relay,
    final,
    gcomp,
    grelay,
    gfinal,
    ext,
    kconv,
    w_sem,
    s1_send,
    s1_recv,
    s2_send,
    f_recv,
    o_sem,
):
    n, nsp, ns, nd, pos, heads, hl, dk, taps = dims
    chunks = [(kv, r) for kv in range(2) for r in range(SPLIT)]
    C = len(chunks)
    rows = pos // SPLIT
    length = nsp * pos
    t = lax.axis_index("tp")
    p = lax.axis_index("sp")
    high = (2 * t) // n
    direction = 1 - 2 * high
    targets = [lax.rem(t + direction * (1 + k) + n, n) for k in range(n)]

    barrier = pltpu.get_barrier_semaphore()
    for k in range(n - 1):
        pl.semaphore_signal(barrier, inc=1, device_id={"tp": targets[k]}, device_id_type=MESH)
    for k in range(nsp - 1):
        pl.semaphore_signal(
            barrier, inc=1, device_id={"sp": lax.rem(p + 1 + k, nsp)}, device_id_type=MESH
        )

    def weight_copy(k, kv):
        columns = pl.ds(pl.multiple_of(targets[k] * (hl * dk), dk), hl * dk)
        source = wv_ref if kv else wk_ref
        return pltpu.make_async_copy(source.at[:, columns], wbuf.at[k, kv], w_sem.at[k, kv])

    for k in range(n):
        for kv in range(2):
            weight_copy(k, kv).start()

    gain = gain_ref[...].astype(jnp.float32)
    step = 32
    for i in range(ns):

        @pl.loop(0, pos // step)
        def _(at):
            window = pl.ds(pl.multiple_of(at * step, step), step)
            wide = x_ref[i, window, :].astype(jnp.float32)
            mean = jnp.mean(wide * wide, axis=-1, keepdims=True)
            normed[i, window, :] = (wide * lax.rsqrt(mean + epsilon) * gain).astype(jnp.bfloat16)

    for i in range(ns):
        for at, w in enumerate((wi_ref, wf_ref)):
            g = lax.dot_general(
                w[...], normed[i], (((0,), (1,)), ((), ())), preferred_element_type=jnp.float32
            )
            gcomp[i, at * heads : (at + 1) * heads, :] = g.astype(jnp.bfloat16)

    def part(buf, lead, c):
        kv, r = chunks[c]
        return buf.at[(*lead, kv, slice(None), pl.ds(r * rows, rows), slice(None))]

    def s1_source(k, i, c):
        return gcomp.at[i] if c == C else part(comp, (k, i), c)

    def s1_target(b, i, c):
        return grelay.at[b, i] if c == C else part(relay, (b, i), c)

    def s1_copy(k, i, c):
        return pltpu.make_async_remote_copy(
            src_ref=s1_source(k, i, c),
            dst_ref=s1_target(t, i, c),
            send_sem=s1_send.at[k, i, c],
            recv_sem=s1_recv.at[t, i, c],
            device_id={"tp": targets[k]},
            device_id_type=MESH,
        )

    def f_target(d, at, c):
        if c == C:
            return gfinal.at[d, at]
        kv, r = chunks[c]
        window = pl.ds(pl.multiple_of(at * pos + r * rows, rows), rows)
        return final.at[d, kv, :, window, :]

    def forward(k, b, i, c, begin):
        s = b * ns + i
        q = s // nd
        d = lax.rem(s, nd)
        source = s1_source(n - 1, i, c) if k == n - 1 else s1_target(b, i, c)
        remote = pltpu.make_async_remote_copy(
            src_ref=source,
            dst_ref=f_target(d, p, c),
            send_sem=s2_send.at[k, i, c],
            recv_sem=f_recv.at[d, p, c],
            device_id={"sp": q},
            device_id_type=MESH,
        )

        @pl.when(q != p)
        def _():
            if begin:
                remote.start()
            else:
                remote.wait_send()

        if begin:

            @pl.when(q == p)
            def _():
                pltpu.make_async_copy(source, f_target(d, p, c), f_recv.at[d, p, c]).start()

    def compute(k):
        for kv in range(2):
            weight_copy(k, kv).wait()
            for i in range(ns):
                y = jnp.dot(normed[i], wbuf[k, kv], preferred_element_type=jnp.float32)
                for h in range(hl):
                    comp[k, i, kv, h] = y[:, h * dk : (h + 1) * dk].astype(jnp.bfloat16)
            if k == 0 and kv == 0:
                pl.semaphore_wait(barrier, n - 1 + nsp - 1)
                for i in range(ns):
                    for to in range(n - 1):
                        s1_copy(to, i, C).start()
                    forward(n - 1, t, i, C, True)
            for i in range(ns):
                for c in range(C):
                    if chunks[c][0] == kv:
                        if k == n - 1:
                            forward(k, t, i, c, True)
                        else:
                            s1_copy(k, i, c).start()

    for k in range(n):
        compute(k)

    def origin(k):
        lower = k + (k >= t).astype(jnp.int32)
        upper = n - 1 - (k + (k >= n - 1 - t).astype(jnp.int32))
        return jnp.where(high == 0, lower, upper)

    def relay_step(k, c):
        b = origin(k)
        for i in range(ns):
            place = s1_target(b, i, c)
            pltpu.make_async_copy(place, place, s1_recv.at[b, i, c]).wait()
            forward(k, b, i, c, True)

    for k in range(n - 1):
        relay_step(k, C)
    for k in range(n - 1):
        for c in range(C):
            relay_step(k, c)

    def arrived(d, at, c):
        place = f_target(d, at, c)
        pltpu.make_async_copy(place, place, f_recv.at[d, at, c]).wait()

    scaling = dk ** (-0.5)
    lane = lax.broadcasted_iota(jnp.int32, (8, length), 1)
    row = lax.broadcasted_iota(jnp.int32, (2 * heads, pos), 0)
    weights, fresh = {}, {}
    for d in range(nd):
        for at in range(nsp):
            arrived(d, at, C)
        for h in range(hl):

            def gate(base):
                pieces = [
                    jnp.sum(
                        jnp.where(
                            row == base + t * hl + h, gfinal[d, at].astype(jnp.float32), 0.0
                        ),
                        axis=0,
                        keepdims=True,
                    )
                    for at in range(nsp)
                ]
                return jnp.concatenate(pieces, axis=1)

            log_forget = log_sigmoid(gate(heads) + fshift_ref[d, h : h + 1, :])
            suffix = pltpu.roll(jnp.broadcast_to(log_forget, (8, length)), length - 1, 1)
            suffix = jnp.where(lane < length - 1, suffix, 0.0)
            hop = 1
            while hop < length:
                moved = pltpu.roll(suffix, length - hop, 1)
                suffix = suffix + jnp.where(lane < length - hop, moved, 0.0)
                hop *= 2
            new_input = ninput_ref[d : d + 1, h : h + 1]
            decay = log_sigmoid(nforget_ref[d : d + 1, h : h + 1])
            log_weight = gate(0) + ishift_ref[d, h : h + 1, :] + suffix + decay
            largest = jnp.maximum(jnp.max(log_weight, axis=1, keepdims=True), new_input)
            weight = jnp.exp(log_weight - largest)
            weight_out[d, h : h + 1, :] = weight[0:1]
            query = query_ref[d, h : h + 1, :].astype(jnp.float32)
            match = jnp.sum(
                nkey_ref[d, h : h + 1, :].astype(jnp.float32) * query, axis=1, keepdims=True
            )
            score = jnp.exp(new_input - largest) * match * scaling
            fresh[d, h] = score.astype(jnp.bfloat16).astype(jnp.float32)
            weights[d, h] = weight

    def key_copy(d, at):
        window = pl.ds(at * pos, pos)
        return pltpu.make_async_copy(
            kconv.at[d, :, window, :], keys_out.at[d, :, window, :], o_sem.at[d, at, C]
        )

    def value_copy(d, at, c):
        r = chunks[c][1]
        window = pl.ds(at * pos + r * rows, rows)
        return pltpu.make_async_copy(
            final.at[d, 1, :, window, :], values_out.at[d, :, window, :], o_sem.at[d, at, c]
        )

    for d in range(nd):
        ext[:, 0:8, :] = jnp.zeros((hl, 8, dk), jnp.float32)
        for at in range(nsp):
            for c in range(C):
                if chunks[c][0] == 0:
                    arrived(d, at, c)
            for h in range(hl):
                ext[h, 8 + at * pos : 8 + (at + 1) * pos, :] = final[
                    d, 0, h, at * pos : (at + 1) * pos, :
                ].astype(jnp.float32)
                tap = conv_ref[
                    :, pl.ds(pl.multiple_of((t * hl + h) * dk, dk), dk)
                ]
                summed = None
                for o in range(taps):
                    start = 8 - (taps - 1) + o + at * pos
                    term = ext[h, start : start + pos, :] * tap[o : o + 1, :]
                    summed = term if summed is None else summed + term
                kconv[d, h, at * pos : (at + 1) * pos, :] = jax.nn.silu(summed).astype(
                    jnp.bfloat16
                )
            key_copy(d, at).start()
        scores = []
        for h in range(hl):
            query = jnp.broadcast_to(query_ref[d, h : h + 1, :], (8, dk))
            matched = lax.dot_general(
                query, kconv[d, h], (((1,), (1,)), ((), ())), preferred_element_type=jnp.float32
            )
            scores.append((weights[d, h] * matched * scaling).astype(jnp.bfloat16))
        for at in range(nsp):
            for c in range(C):
                if chunks[c][0] == 1:
                    arrived(d, at, c)
                    value_copy(d, at, c).start()
        for h in range(hl):
            score = scores[h]
            denominator = jnp.sum(score.astype(jnp.float32), axis=1, keepdims=True) + fresh[d, h]
            numerator = jnp.dot(score, final[d, 1, h], preferred_element_type=jnp.float32)
            numerator = numerator + fresh[d, h] * nvalue_ref[d, h : h + 1, :].astype(jnp.float32)
            result = numerator / jnp.maximum(jnp.abs(denominator), 1.0)
            read_out[d, h : h + 1, :] = result[0:1].astype(jnp.bfloat16)

    for k in range(n):
        b = t if k == n - 1 else origin(k)
        for i in range(ns):
            for c in range(C + 1):
                if k < n - 1:
                    s1_copy(k, i, c).wait_send()
                forward(k, b, i, c, False)
    for d in range(nd):
        for at in range(nsp):
            key_copy(d, at).wait()
            for c in range(C):
                if chunks[c][0] == 1:
                    value_copy(d, at, c).wait()


def shards(
    n,
    nsp,
    layer_input,
    norm_gain,
    key_weight,
    value_weight,
    input_gate_weight,
    forget_gate_weight,
    conv_weight,
    input_shift,
    forget_shift,
    new_query,
    new_key,
    new_value,
    new_input,
    new_forget,
):
    ns, pos, width = layer_input.shape
    nd, hl, length = input_shift.shape
    dk = new_query.shape[2]
    heads = input_gate_weight.shape[1]
    taps = conv_weight.shape[0]
    dims = (n, nsp, ns, nd, pos, heads, hl, dk, taps)
    C = 2 * SPLIT
    bf16, f32 = jnp.bfloat16, jnp.float32
    vmem = pl.BlockSpec(memory_space=pltpu.VMEM)
    hbm = pl.BlockSpec(memory_space=pl.ANY)
    dma = pltpu.SemaphoreType.DMA
    return pl.pallas_call(
        functools.partial(kernel, dims),
        out_shape=(
            jax.ShapeDtypeStruct((nd, hl, length, dk), bf16),
            jax.ShapeDtypeStruct((nd, hl, length, dk), bf16),
            jax.ShapeDtypeStruct((nd, hl, length), f32),
            jax.ShapeDtypeStruct((nd, hl, dk), bf16),
        ),
        in_specs=[vmem] * 12 + [hbm] * 2,
        out_specs=(hbm, hbm, vmem, vmem),
        scratch_shapes=[
            pltpu.VMEM((n, 2, width, hl * dk), bf16),
            pltpu.VMEM((ns, pos, width), bf16),
            pltpu.VMEM((n, ns, 2, hl, pos, dk), bf16),
            pltpu.VMEM((n, ns, 2, hl, pos, dk), bf16),
            pltpu.VMEM((nd, 2, hl, length, dk), bf16),
            pltpu.VMEM((ns, 2 * heads, pos), bf16),
            pltpu.VMEM((n, ns, 2 * heads, pos), bf16),
            pltpu.VMEM((nd, nsp, 2 * heads, pos), bf16),
            pltpu.VMEM((hl, 8 + length, dk), f32),
            pltpu.VMEM((nd, hl, length, dk), bf16),
            dma((n, 2)),
            dma((n, ns, C + 1)),
            dma((n, ns, C + 1)),
            dma((n, ns, C + 1)),
            dma((nd, nsp, C + 1)),
            dma((nd, nsp, C + 1)),
        ],
        compiler_params=pltpu.CompilerParams(
            collective_id=0, has_side_effects=True, vmem_limit_bytes=60 * 1024 * 1024
        ),
    )(
        layer_input,
        norm_gain.reshape(1, width),
        input_gate_weight,
        forget_gate_weight,
        conv_weight,
        input_shift,
        forget_shift,
        new_query,
        new_key,
        new_value,
        new_input,
        new_forget,
        key_weight,
        value_weight,
    )


def solution(mesh):
    in_specs = (
        P(("grp", "tp"), "sp", None),
        P(),
        P(),
        P(),
        P(),
        P(),
        P(),
        P(("grp", "sp"), "tp", None),
        P(("grp", "sp"), "tp", None),
        P(("grp", "sp"), "tp", None),
        P(("grp", "sp"), "tp", None),
        P(("grp", "sp"), "tp", None),
        P(("grp", "sp"), "tp"),
        P(("grp", "sp"), "tp"),
    )
    out_specs = (
        P(("grp", "sp"), "tp", None, None),
        P(("grp", "sp"), "tp", None, None),
        P(("grp", "sp"), "tp", None),
        P(("grp", "sp"), "tp", None),
    )
    body = functools.partial(shards, mesh.shape["tp"], mesh.shape["sp"])
    return jax.shard_map(body, mesh=mesh, in_specs=in_specs, out_specs=out_specs, check_vma=False)
```

time: 107 us -> 53.4 us (0.50)
  waiting for transfers between devices: 48.4 us -> 0 us
  Pallas kernels: 0 us -> 41.1 us
  starting transfers between devices: 33.8 us -> 0 us
  matrix products: 10.3 us -> 0 us
  other arithmetic: 9.68 us -> 0 us
  local copies, waits for them, and re-layouts: 3.49 us -> 11 us
    all_to_all x8 -> x0, waiting for transfers between devices: 47.6 us -> none  [the longest x1 11.6 us: shards(): lax.all_to_all(keys, 'tp', split_axis=1, concat_axis=0, tiled=True)]
    pallas_call x0 -> x1, Pallas kernels: none -> 41.1 us  [shards(): pl.pallas_call(functools.partial(kernel, dims), out_shape=(jax.ShapeDtype...]
    all_to_all x8 -> x0, starting transfers between devices: 31.4 us -> none  [the longest x1 6.35 us: shards(): lax.all_to_all(forget_linear, 'tp', split_axis=1, concat_axis=0, tiled=True)]
    dot_general x6 -> x0, matrix products: 10.3 us -> none  [the longest x1 4.29 us: project_rows(): jnp.einsum('apd,dhk->ahpk', normed, value_matrix, preferred_element_type=...]
    unnamed x32 -> x6, local copies, waits for them, and re-layouts: 1.83 us -> 9.69 us
    convert_element_type x6 -> x0, other arithmetic: 2.95 us -> none  [the longest x1 1.46 us: convolve(): return jax.nn.silu(summed).astype(jnp.bfloat16)]
    another operation x2 -> x0, other arithmetic: 2.68 us -> none
    reduce_sum x3 -> x0, other arithmetic: 2.43 us -> none  [the longest x1 1.51 us: project_rows(): jnp.mean(widened * widened, axis=-1, keepdims=True) + epsilon]
  transfers between devices with their start and end apart: 9 -> 0, of which waited for: 8 -> 0; matrix products, arithmetic and copies ran while one was open for 14% -> 0% of each run, Pallas kernels for 0% -> 0%
where the time goes in v1:
time: 53.4 us; the launch traced here: 52.7 us
  Pallas kernels  41.1 us (77%)
  local copies, waits for them, and re-layouts  11 us (21%)
  between operations  0.64 us (1%)
    pallas_call x1, Pallas kernels, shards(): pl.pallas_call(functools.partial(kernel, dims), out_shape=(jax.ShapeDtype...  41.1 us
    unnamed x6, local copies, waits for them, and re-layouts  9.69 us
    reshape x1, local copies, waits for them, and re-layouts, shards(): norm_gain.reshape(1, width)  1.29 us

profile of v1, /device:TPU:0, one launch (start us, length us, event | category | flops | bytes accessed | tf_op | source)
XLA Modules:
  0.0 52.7 jit_solution(16460578148854846262)
XLA Ops:
  0.6 1.3 %reshape.11.gain_ref = bf16[1,2048]{1,0:T(2,128)(2,1)} reshape(bf16[2048]{0:T(1024)(128)(2,1)} %param.15) | data formatting | bytes 8192 | tf_op jit(solution)/shard_map/reshape | solution.py:378
  1.9 1.8 %copy.18.wi_ref = bf16[2048,8]{1,0:T(8,128)(2,1)} copy(bf16[2048,8]{0,1:T(8,128)(2,1)} %param.18) | data formatting | bytes 65536 | tf_op args[4]
  3.7 1.8 %copy.19.wf_ref = bf16[2048,8]{1,0:T(8,128)(2,1)} copy(bf16[2048,8]{0,1:T(8,128)(2,1)} %param.19) | data formatting | bytes 65536 | tf_op args[5]
  5.4 41.1 %shard_map.165 = (bf16[1,2,1024,128]{3,2,1,0:T(8,128)(2,1)}, bf16[1,2,1024,128]{3,2,1,0:T(8,128)(2,1)}, f32[1,2,1024]{2,1,0:T(2,128)}, bf16[1,2,128]{2,1,0:T(2,128)(2,1)}) custom-call(bf16[1,256,2048]{2,1,0:T(8,128)(2,1)} %x_ref.1, bf16[1,2048]{1,0:T(2,128)(2,1)} %reshape.11.gain_ref, bf16[2048,8]{1,0:T(8,128)(2,1)} %copy.18.wi_ref, ...), custom_call_target="tpu_custom_call" | custom-call | tf_op jit(solution)/shard_map/pallas_call | solution.py:345
  46.6 1.9 %copy.24 = bf16[1,2,1024,128]{3,2,1,0:T(8,128)(2,1)} copy(bf16[1,2,1024,128]{3,2,1,0:T(8,128)(2,1)} %get-tuple-element.8) | data formatting | bytes 1048576
  48.4 1.9 %copy.25 = bf16[1,2,1024,128]{3,2,1,0:T(8,128)(2,1)} copy(bf16[1,2,1024,128]{3,2,1,0:T(8,128)(2,1)} %get-tuple-element.9) | data formatting | bytes 1048576
  50.3 1.3 %copy.26 = f32[1,2,1024]{2,1,0:T(2,128)} copy(f32[1,2,1024]{2,1,0:T(2,128)} %get-tuple-element.10) | data formatting | bytes 16384
  51.6 1.1 %copy.27 = bf16[1,2,128]{2,1,0:T(2,128)(2,1)} copy(bf16[1,2,128]{2,1,0:T(2,128)(2,1)} %get-tuple-element.11) | data formatting | bytes 1024

commit v2 on v1

--- a/solution.py
+++ b/solution.py
@@ -45,13 +45,11 @@
     grelay,
     gfinal,
     ext,
-    kconv,
     w_sem,
     s1_send,
     s1_recv,
     s2_send,
     f_recv,
-    o_sem,
 ):
     n, nsp, ns, nd, pos, heads, hl, dk, taps = dims
     chunks = [(kv, r) for kv in range(2) for r in range(SPLIT)]
@@ -81,7 +79,7 @@
         for kv in range(2):
             weight_copy(k, kv).start()
 
-    gain = gain_ref[...].astype(jnp.float32)
+    gain = gain_ref[...].astype(jnp.float32).reshape(1, -1)
     step = 32
     for i in range(ns):
 
@@ -91,13 +89,6 @@
             wide = x_ref[i, window, :].astype(jnp.float32)
             mean = jnp.mean(wide * wide, axis=-1, keepdims=True)
             normed[i, window, :] = (wide * lax.rsqrt(mean + epsilon) * gain).astype(jnp.bfloat16)
-
-    for i in range(ns):
-        for at, w in enumerate((wi_ref, wf_ref)):
-            g = lax.dot_general(
-                w[...], normed[i], (((0,), (1,)), ((), ())), preferred_element_type=jnp.float32
-            )
-            gcomp[i, at * heads : (at + 1) * heads, :] = g.astype(jnp.bfloat16)
 
     def part(buf, lead, c):
         kv, r = chunks[c]
@@ -124,7 +115,7 @@
             return gfinal.at[d, at]
         kv, r = chunks[c]
         window = pl.ds(pl.multiple_of(at * pos + r * rows, rows), rows)
-        return final.at[d, kv, :, window, :]
+        return (values_out if kv else final).at[d, :, window, :]
 
     def forward(k, b, i, c, begin):
         s = b * ns + i
@@ -162,10 +153,6 @@
                     comp[k, i, kv, h] = y[:, h * dk : (h + 1) * dk].astype(jnp.bfloat16)
             if k == 0 and kv == 0:
                 pl.semaphore_wait(barrier, n - 1 + nsp - 1)
-                for i in range(ns):
-                    for to in range(n - 1):
-                        s1_copy(to, i, C).start()
-                    forward(n - 1, t, i, C, True)
             for i in range(ns):
                 for c in range(C):
                     if chunks[c][0] == kv:
@@ -174,8 +161,21 @@
                         else:
                             s1_copy(k, i, c).start()
 
+    def gates():
+        for i in range(ns):
+            for at, w in enumerate((wi_ref, wf_ref)):
+                g = lax.dot_general(
+                    w[...], normed[i], (((1,), (1,)), ((), ())), preferred_element_type=jnp.float32
+                )
+                gcomp[i, at * heads : (at + 1) * heads, :] = g.astype(jnp.bfloat16)
+            for to in range(n - 1):
+                s1_copy(to, i, C).start()
+            forward(n - 1, t, i, C, True)
+
     for k in range(n):
         compute(k)
+        if k == 0:
+            gates()
 
     def origin(k):
         lower = k + (k >= t).astype(jnp.int32)
@@ -191,7 +191,6 @@
 
     for k in range(n - 1):
         relay_step(k, C)
-    for k in range(n - 1):
         for c in range(C):
             relay_step(k, c)
 
@@ -243,19 +242,6 @@
             fresh[d, h] = score.astype(jnp.bfloat16).astype(jnp.float32)
             weights[d, h] = weight
 
-    def key_copy(d, at):
-        window = pl.ds(at * pos, pos)
-        return pltpu.make_async_copy(
-            kconv.at[d, :, window, :], keys_out.at[d, :, window, :], o_sem.at[d, at, C]
-        )
-
-    def value_copy(d, at, c):
-        r = chunks[c][1]
-        window = pl.ds(at * pos + r * rows, rows)
-        return pltpu.make_async_copy(
-            final.at[d, 1, :, window, :], values_out.at[d, :, window, :], o_sem.at[d, at, c]
-        )
-
     for d in range(nd):
         ext[:, 0:8, :] = jnp.zeros((hl, 8, dk), jnp.float32)
         for at in range(nsp):
@@ -264,7 +250,7 @@
                     arrived(d, at, c)
             for h in range(hl):
                 ext[h, 8 + at * pos : 8 + (at + 1) * pos, :] = final[
-                    d, 0, h, at * pos : (at + 1) * pos, :
+                    d, h, at * pos : (at + 1) * pos, :
                 ].astype(jnp.float32)
                 tap = conv_ref[
                     :, pl.ds(pl.multiple_of((t * hl + h) * dk, dk), dk)
@@ -274,26 +260,24 @@
                     start = 8 - (taps - 1) + o + at * pos
                     term = ext[h, start : start + pos, :] * tap[o : o + 1, :]
                     summed = term if summed is None else summed + term
-                kconv[d, h, at * pos : (at + 1) * pos, :] = jax.nn.silu(summed).astype(
+                keys_out[d, h, at * pos : (at + 1) * pos, :] = jax.nn.silu(summed).astype(
                     jnp.bfloat16
                 )
-            key_copy(d, at).start()
         scores = []
         for h in range(hl):
             query = jnp.broadcast_to(query_ref[d, h : h + 1, :], (8, dk))
             matched = lax.dot_general(
-                query, kconv[d, h], (((1,), (1,)), ((), ())), preferred_element_type=jnp.float32
+                query, keys_out[d, h], (((1,), (1,)), ((), ())), preferred_element_type=jnp.float32
             )
             scores.append((weights[d, h] * matched * scaling).astype(jnp.bfloat16))
         for at in range(nsp):
             for c in range(C):
                 if chunks[c][0] == 1:
                     arrived(d, at, c)
-                    value_copy(d, at, c).start()
         for h in range(hl):
             score = scores[h]
             denominator = jnp.sum(score.astype(jnp.float32), axis=1, keepdims=True) + fresh[d, h]
-            numerator = jnp.dot(score, final[d, 1, h], preferred_element_type=jnp.float32)
+            numerator = jnp.dot(score, values_out[d, h], preferred_element_type=jnp.float32)
             numerator = numerator + fresh[d, h] * nvalue_ref[d, h : h + 1, :].astype(jnp.float32)
             result = numerator / jnp.maximum(jnp.abs(denominator), 1.0)
             read_out[d, h : h + 1, :] = result[0:1].astype(jnp.bfloat16)
@@ -305,12 +289,17 @@
                 if k < n - 1:
                     s1_copy(k, i, c).wait_send()
                 forward(k, b, i, c, False)
-    for d in range(nd):
-        for at in range(nsp):
-            key_copy(d, at).wait()
-            for c in range(C):
-                if chunks[c][0] == 1:
-                    value_copy(d, at, c).wait()
+
+def write_out(*refs):
+    count = (len(refs) - 1) // 2
+    sem = refs[-1]
+    copies = [
+        pltpu.make_async_copy(refs[i], refs[count + i], sem.at[i]) for i in range(count)
+    ]
+    for copy in copies:
+        copy.start()
+    for copy in copies:
+        copy.wait()
 
 
 def shards(
@@ -340,34 +329,33 @@
     C = 2 * SPLIT
     bf16, f32 = jnp.bfloat16, jnp.float32
     vmem = pl.BlockSpec(memory_space=pltpu.VMEM)
-    hbm = pl.BlockSpec(memory_space=pl.ANY)
+    hbm = pl.BlockSpec(memory_space=pltpu.HBM)
     dma = pltpu.SemaphoreType.DMA
-    return pl.pallas_call(
+    out_shape=(
+        jax.ShapeDtypeStruct((nd, hl, length, dk), bf16),
+        jax.ShapeDtypeStruct((nd, hl, length, dk), bf16),
+        jax.ShapeDtypeStruct((nd, hl, length), f32),
+        jax.ShapeDtypeStruct((nd, hl, dk), bf16),
+    )
+    held = pl.pallas_call(
         functools.partial(kernel, dims),
-        out_shape=(
-            jax.ShapeDtypeStruct((nd, hl, length, dk), bf16),
-            jax.ShapeDtypeStruct((nd, hl, length, dk), bf16),
-            jax.ShapeDtypeStruct((nd, hl, length), f32),
-            jax.ShapeDtypeStruct((nd, hl, dk), bf16),
-        ),
+        out_shape=tuple(pltpu.VMEM(o.shape, o.dtype) for o in out_shape),
         in_specs=[vmem] * 12 + [hbm] * 2,
-        out_specs=(hbm, hbm, vmem, vmem),
+        out_specs=(vmem,) * 4,
         scratch_shapes=[
             pltpu.VMEM((n, 2, width, hl * dk), bf16),
             pltpu.VMEM((ns, pos, width), bf16),
             pltpu.VMEM((n, ns, 2, hl, pos, dk), bf16),
             pltpu.VMEM((n, ns, 2, hl, pos, dk), bf16),
-            pltpu.VMEM((nd, 2, hl, length, dk), bf16),
+            pltpu.VMEM((nd, hl, length, dk), bf16),
             pltpu.VMEM((ns, 2 * heads, pos), bf16),
             pltpu.VMEM((n, ns, 2 * heads, pos), bf16),
             pltpu.VMEM((nd, nsp, 2 * heads, pos), bf16),
             pltpu.VMEM((hl, 8 + length, dk), f32),
-            pltpu.VMEM((nd, hl, length, dk), bf16),
             dma((n, 2)),
             dma((n, ns, C + 1)),
             dma((n, ns, C + 1)),
             dma((n, ns, C + 1)),
-            dma((nd, nsp, C + 1)),
             dma((nd, nsp, C + 1)),
         ],
         compiler_params=pltpu.CompilerParams(
@@ -375,9 +363,9 @@
         ),
     )(
         layer_input,
-        norm_gain.reshape(1, width),
-        input_gate_weight,
-        forget_gate_weight,
+        norm_gain,
+        input_gate_weight.T,
+        forget_gate_weight.T,
         conv_weight,
         input_shift,
         forget_shift,
@@ -389,6 +377,14 @@
         key_weight,
         value_weight,
     )
+    return pl.pallas_call(
+        write_out,
+        out_shape=out_shape,
+        in_specs=[vmem] * len(out_shape),
+        out_specs=(hbm,) * len(out_shape),
+        scratch_shapes=[dma((len(out_shape),))],
+        compiler_params=pltpu.CompilerParams(vmem_limit_bytes=8 * 1024 * 1024),
+    )(*held)
 
 
 def solution(mesh):

time: 53.4 us -> 41.5 us (0.78); the launches traced: 52.7 us -> 41.4 us
  local copies, waits for them, and re-layouts: 11 us -> 0 us
    unnamed x6 -> x0, local copies, waits for them, and re-layouts: 9.69 us -> none
    reshape x1 -> x0, local copies, waits for them, and re-layouts: 1.29 us -> none  [shards(): norm_gain.reshape(1, width)]
    pallas_call x1 -> x2, Pallas kernels: 41.1 us -> 40.7 us  [the longest x1 39.7 us: shards(): pl.pallas_call(functools.partial(kernel, dims), out_shape=tuple((pltpu.VM...]
where the time goes in v2:
time: 41.5 us; the launch traced here: 41.4 us
  Pallas kernels  40.7 us (98%)
  between operations  0.64 us (2%)
    pallas_call x1, Pallas kernels, shards(): pl.pallas_call(functools.partial(kernel, dims), out_shape=tuple((pltpu.VM...  39.7 us
    pallas_call x1, Pallas kernels, shards(): pl.pallas_call(write_out, out_shape=out_shape, in_specs=[vmem] * len(out_...  1.01 us

profile of v2, /device:TPU:0, one launch (start us, length us, event | category | flops | bytes accessed | tf_op | source)
XLA Modules:
  0.0 41.4 jit_solution(3960575680064768155)
XLA Ops:
  0.6 39.7 %shard_map.165 = (bf16[1,2,1024,128]{3,2,1,0:T(8,128)(2,1)S(1)}, bf16[1,2,1024,128]{3,2,1,0:T(8,128)(2,1)S(1)}, f32[1,2,1024]{2,1,0:T(2,128)S(1)}, bf16[1,2,128]{2,1,0:T(2,128)(2,1)S(1)}) custom-call(bf16[1,256,2048]{2,1,0:T(8,128)(2,1)} %x_ref.1, bf16[2048]{0:T(1024)(128)(2,1)} %gain_ref.1, bf16[8,2048]{1,0:T(8,128)(2,1)} %bitcast.2, ...), custom_call_target="tpu_custom_call" | custom-call | tf_op jit(solution)/shard_map/pallas_call | solution.py:340
  40.4 1.0 %shard_map.166 = (bf16[1,2,1024,128]{3,2,1,0:T(8,128)(2,1)}, bf16[1,2,1024,128]{3,2,1,0:T(8,128)(2,1)}, f32[1,2,1024]{2,1,0:T(2,128)}, bf16[1,2,128]{2,1,0:T(2,128)(2,1)}) custom-call(bf16[1,2,1024,128]{3,2,1,0:T(8,128)(2,1)S(1)} %get-tuple-element.8.refs_0_, bf16[1,2,1024,128]{3,2,1,0:T(8,128)(2,1)S(1)} %get-tuple-element.9.refs_1_, ...), custom_call_target="tpu_custom_call" | custom-call | tf_op jit(solution)/shard_map/pallas_call | solution.py:380

commit v3 on v2

--- a/solution.py
+++ b/solution.py
@@ -189,10 +189,6 @@
             pltpu.make_async_copy(place, place, s1_recv.at[b, i, c]).wait()
             forward(k, b, i, c, True)
 
-    for k in range(n - 1):
-        relay_step(k, C)
-        for c in range(C):
-            relay_step(k, c)
 
     def arrived(d, at, c):
         place = f_target(d, at, c)
@@ -202,80 +198,101 @@
     lane = lax.broadcasted_iota(jnp.int32, (8, length), 1)
     row = lax.broadcasted_iota(jnp.int32, (2 * heads, pos), 0)
     weights, fresh = {}, {}
+    scores = {}
+
+    def weigh():
+        for d in range(nd):
+            for at in range(nsp):
+                arrived(d, at, C)
+            for h in range(hl):
+
+                def gate(base):
+                    pieces = [
+                        jnp.sum(
+                            jnp.where(
+                                row == base + t * hl + h, gfinal[d, at].astype(jnp.float32), 0.0
+                            ),
+                            axis=0,
+                            keepdims=True,
+                        )
+                        for at in range(nsp)
+                    ]
+                    return jnp.concatenate(pieces, axis=1)
+
+                log_forget = log_sigmoid(gate(heads) + fshift_ref[d, h : h + 1, :])
+                suffix = pltpu.roll(jnp.broadcast_to(log_forget, (8, length)), length - 1, 1)
+                suffix = jnp.where(lane < length - 1, suffix, 0.0)
+                hop = 1
+                while hop < length:
+                    moved = pltpu.roll(suffix, length - hop, 1)
+                    suffix = suffix + jnp.where(lane < length - hop, moved, 0.0)
+                    hop *= 2
+                new_input = ninput_ref[d : d + 1, h : h + 1]
+                decay = log_sigmoid(nforget_ref[d : d + 1, h : h + 1])
+                log_weight = gate(0) + ishift_ref[d, h : h + 1, :] + suffix + decay
+                largest = jnp.maximum(jnp.max(log_weight, axis=1, keepdims=True), new_input)
+                weight = jnp.exp(log_weight - largest)
+                weight_out[d, h : h + 1, :] = weight[0:1]
+                query = query_ref[d, h : h + 1, :].astype(jnp.float32)
+                match = jnp.sum(
+                    nkey_ref[d, h : h + 1, :].astype(jnp.float32) * query, axis=1, keepdims=True
+                )
+                score = jnp.exp(new_input - largest) * match * scaling
+                fresh[d, h] = score.astype(jnp.bfloat16).astype(jnp.float32)
+                weights[d, h] = weight
+
+
+    def convolve():
+        for d in range(nd):
+            ext[:, 0:8, :] = jnp.zeros((hl, 8, dk), jnp.float32)
+            for at in range(nsp):
+                for c in range(C):
+                    if chunks[c][0] == 0:
+                        arrived(d, at, c)
+                for h in range(hl):
+                    ext[h, 8 + at * pos : 8 + (at + 1) * pos, :] = final[
+                        d, h, at * pos : (at + 1) * pos, :
+                    ].astype(jnp.float32)
+                    tap = conv_ref[
+                        :, pl.ds(pl.multiple_of((t * hl + h) * dk, dk), dk)
+                    ]
+                    summed = None
+                    for o in range(taps):
+                        start = 8 - (taps - 1) + o + at * pos
+                        term = ext[h, start : start + pos, :] * tap[o : o + 1, :]
+                        summed = term if summed is None else summed + term
+                    keys_out[d, h, at * pos : (at + 1) * pos, :] = jax.nn.silu(summed).astype(
+                        jnp.bfloat16
+                    )
+            for h in range(hl):
+                query = jnp.broadcast_to(query_ref[d, h : h + 1, :], (8, dk))
+                matched = lax.dot_general(
+                    query, keys_out[d, h], (((1,), (1,)), ((), ())), preferred_element_type=jnp.float32
+                )
+                scores[d, h] = (weights[d, h] * matched * scaling).astype(jnp.bfloat16)
+
+    for k in range(n - 1):
+        relay_step(k, C)
+    for k in range(n - 1):
+        for c in range(C):
+            if k == n - 2 and c == C - 1:
+                if n == 2:
+                    weigh()
+                convolve()
+            relay_step(k, c)
+        if k == 0 and n > 2:
+            weigh()
+    if n == 1:
+        weigh()
+        convolve()
+
     for d in range(nd):
-        for at in range(nsp):
-            arrived(d, at, C)
-        for h in range(hl):
-
-            def gate(base):
-                pieces = [
-                    jnp.sum(
-                        jnp.where(
-                            row == base + t * hl + h, gfinal[d, at].astype(jnp.float32), 0.0
-                        ),
-                        axis=0,
-                        keepdims=True,
-                    )
-                    for at in range(nsp)
-                ]
-                return jnp.concatenate(pieces, axis=1)
-
-            log_forget = log_sigmoid(gate(heads) + fshift_ref[d, h : h + 1, :])
-            suffix = pltpu.roll(jnp.broadcast_to(log_forget, (8, length)), length - 1, 1)
-            suffix = jnp.where(lane < length - 1, suffix, 0.0)
-            hop = 1
-            while hop < length:
-                moved = pltpu.roll(suffix, length - hop, 1)
-                suffix = suffix + jnp.where(lane < length - hop, moved, 0.0)
-                hop *= 2
-            new_input = ninput_ref[d : d + 1, h : h + 1]
-            decay = log_sigmoid(nforget_ref[d : d + 1, h : h + 1])
-            log_weight = gate(0) + ishift_ref[d, h : h + 1, :] + suffix + decay
-            largest = jnp.maximum(jnp.max(log_weight, axis=1, keepdims=True), new_input)
-            weight = jnp.exp(log_weight - largest)
-            weight_out[d, h : h + 1, :] = weight[0:1]
-            query = query_ref[d, h : h + 1, :].astype(jnp.float32)
-            match = jnp.sum(
-                nkey_ref[d, h : h + 1, :].astype(jnp.float32) * query, axis=1, keepdims=True
-            )
-            score = jnp.exp(new_input - largest) * match * scaling
-            fresh[d, h] = score.astype(jnp.bfloat16).astype(jnp.float32)
-            weights[d, h] = weight
-
-    for d in range(nd):
-        ext[:, 0:8, :] = jnp.zeros((hl, 8, dk), jnp.float32)
-        for at in range(nsp):
-            for c in range(C):
-                if chunks[c][0] == 0:
-                    arrived(d, at, c)
-            for h in range(hl):
-                ext[h, 8 + at * pos : 8 + (at + 1) * pos, :] = final[
-                    d, h, at * pos : (at + 1) * pos, :
-                ].astype(jnp.float32)
-                tap = conv_ref[
-                    :, pl.ds(pl.multiple_of((t * hl + h) * dk, dk), dk)
-                ]
-                summed = None
-                for o in range(taps):
-                    start = 8 - (taps - 1) + o + at * pos
-                    term = ext[h, start : start + pos, :] * tap[o : o + 1, :]
-                    summed = term if summed is None else summed + term
-                keys_out[d, h, at * pos : (at + 1) * pos, :] = jax.nn.silu(summed).astype(
-                    jnp.bfloat16
-                )
-        scores = []
-        for h in range(hl):
-            query = jnp.broadcast_to(query_ref[d, h : h + 1, :], (8, dk))
-            matched = lax.dot_general(
-                query, keys_out[d, h], (((1,), (1,)), ((), ())), preferred_element_type=jnp.float32
-            )
-            scores.append((weights[d, h] * matched * scaling).astype(jnp.bfloat16))
         for at in range(nsp):
             for c in range(C):
                 if chunks[c][0] == 1:
                     arrived(d, at, c)
         for h in range(hl):
-            score = scores[h]
+            score = scores[d, h]
             denominator = jnp.sum(score.astype(jnp.float32), axis=1, keepdims=True) + fresh[d, h]
             numerator = jnp.dot(score, values_out[d, h], preferred_element_type=jnp.float32)
             numerator = numerator + fresh[d, h] * nvalue_ref[d, h : h + 1, :].astype(jnp.float32)

time: 41.5 us -> 41.4 us (level)
  no operation moved by 1% of the time
where the time goes in v3:
time: 41.4 us; the launch traced here: 41.2 us
  Pallas kernels  40.6 us (98%)
  between operations  0.64 us (2%)
    pallas_call x1, Pallas kernels, shards(): pl.pallas_call(functools.partial(kernel, dims), out_shape=tuple((pltpu.VM...  39.6 us
    pallas_call x1, Pallas kernels, shards(): pl.pallas_call(write_out, out_shape=out_shape, in_specs=[vmem] * len(out_...  1.01 us

profile of v3, /device:TPU:0, one launch (start us, length us, event | category | flops | bytes accessed | tf_op | source)
XLA Modules:
  0.0 41.2 jit_solution(2806875786857468140)
XLA Ops:
  0.6 39.6 %shard_map.165 = (bf16[1,2,1024,128]{3,2,1,0:T(8,128)(2,1)S(1)}, bf16[1,2,1024,128]{3,2,1,0:T(8,128)(2,1)S(1)}, f32[1,2,1024]{2,1,0:T(2,128)S(1)}, bf16[1,2,128]{2,1,0:T(2,128)(2,1)S(1)}) custom-call(bf16[1,256,2048]{2,1,0:T(8,128)(2,1)} %x_ref.1, bf16[2048]{0:T(1024)(128)(2,1)} %gain_ref.1, bf16[8,2048]{1,0:T(8,128)(2,1)} %bitcast.2, ...), custom_call_target="tpu_custom_call" | custom-call | tf_op jit(solution)/shard_map/pallas_call | solution.py:357
  40.2 1.0 %shard_map.166 = (bf16[1,2,1024,128]{3,2,1,0:T(8,128)(2,1)}, bf16[1,2,1024,128]{3,2,1,0:T(8,128)(2,1)}, f32[1,2,1024]{2,1,0:T(2,128)}, bf16[1,2,128]{2,1,0:T(2,128)(2,1)}) custom-call(bf16[1,2,1024,128]{3,2,1,0:T(8,128)(2,1)S(1)} %get-tuple-element.8.refs_0_, bf16[1,2,1024,128]{3,2,1,0:T(8,128)(2,1)S(1)} %get-tuple-element.9.refs_1_, ...), custom_call_target="tpu_custom_call" | custom-call | tf_op jit(solution)/shard_map/pallas_call | solution.py:397
